TPU v7x, 32 devices: a whole 2x2x4 slice. The times are simulated.
32 devices in a mesh: fs: 8 (over z, x), tp: 4 (over y, core).
Axes of the slice: x: 2, y: 2, z: 4, core: 2. Of those that a mesh axis runs over, the one named last changes fastest.
Arguments:
- prompts: bfloat16 [4, 1024, 2048], P('tp'), may hold values from -6 to 6
- gain_first: float32 [2048], P('fs'), may hold values from 0.1 to 1.9
- gate_first: float32 [2048, 5632], P('fs', 'tp'), may hold values from -0.125 to 0.125
- up_first: float32 [2048, 5632], P('fs', 'tp'), may hold values from -0.125 to 0.125
- down_first: float32 [5632, 2048], P('fs', 'tp'), may hold values from -0.078125 to 0.078125
- gain_second: float32 [2048], P('fs'), may hold values from 0.1 to 1.9
- gate_second: float32 [2048, 5632], P('fs', 'tp'), may hold values from -0.125 to 0.125
- up_second: float32 [2048, 5632], P('fs', 'tp'), may hold values from -0.125 to 0.125
- down_second: float32 [5632, 2048], P('fs', 'tp'), may hold values from -0.078125 to 0.078125
Outputs:
- served_gate_first: bfloat16 [2048, 5632], P(None, 'fs')
- served_up_first: bfloat16 [2048, 5632], P(None, 'fs')
- served_down_first: bfloat16 [5632, 2048], P('fs')
- served_gate_second: bfloat16 [2048, 5632], P(None, 'fs')
- served_up_second: bfloat16 [2048, 5632], P(None, 'fs')
- served_down_second: bfloat16 [5632, 2048], P('fs')
- prompt_states: bfloat16 [4, 1024, 2048], P('tp', 'fs')
All inputs are finite; a program needn't handle non-finite values.
Results may differ from a plain program's by a relative error of at most 0.012.
Values may be sent and summed in bfloat16 or wider, within the bound.
A program may use at most 128 MiB of HBM per device.

v0:
```python
import jax
import jax.numpy as jnp
from jax import lax
from jax.sharding import PartitionSpec as P


def normalize(row_block):
    widened = row_block.astype(jnp.float32)
    scaled = widened * lax.rsqrt(jnp.mean(widened * widened, axis=-1, keepdims=True) + 1e-06)
    return scaled.astype(jnp.bfloat16)


def activate(normed, gate_cols, up_cols):
    gate_val = jnp.dot(normed, gate_cols, preferred_element_type=jnp.float32)
    up_val = jnp.dot(normed, up_cols, preferred_element_type=jnp.float32)
    return (jax.nn.silu(gate_val) * up_val).astype(jnp.bfloat16)


def reorder(matrix, outer_count, inner_count):
    total_rows, columns = matrix.shape
    block_rows = total_rows // (outer_count * inner_count)
    shaped = matrix.reshape(outer_count, inner_count, block_rows, columns)
    return jnp.transpose(shaped, (1, 0, 2, 3)).reshape(total_rows, columns)


def per_device(
    prompts,
    gain_first,
    gate_first,
    up_first,
    down_first,
    gain_second,
    gate_second,
    up_second,
    down_second,
):
    fold_gate_a = (gain_first[:, None] * gate_first).astype(jnp.bfloat16)
    fold_up_a = (gain_first[:, None] * up_first).astype(jnp.bfloat16)
    fold_gate_b = (gain_second[:, None] * gate_second).astype(jnp.bfloat16)
    fold_up_b = (gain_second[:, None] * up_second).astype(jnp.bfloat16)
    round_down_a = down_first.astype(jnp.bfloat16)
    round_down_b = down_second.astype(jnp.bfloat16)
    sliced = (
        lax.all_to_all(fold_gate_a, "tp", split_axis=0, concat_axis=1, tiled=True),
        lax.all_to_all(fold_up_a, "tp", split_axis=0, concat_axis=1, tiled=True),
        lax.all_to_all(fold_gate_b, "tp", split_axis=0, concat_axis=1, tiled=True),
        lax.all_to_all(fold_up_b, "tp", split_axis=0, concat_axis=1, tiled=True),
    )
    blocked = (
        lax.all_to_all(sliced[0], "fs", split_axis=1, concat_axis=0, tiled=True),
        lax.all_to_all(sliced[1], "fs", split_axis=1, concat_axis=0, tiled=True),
        lax.all_to_all(sliced[2], "fs", split_axis=1, concat_axis=0, tiled=True),
        lax.all_to_all(sliced[3], "fs", split_axis=1, concat_axis=0, tiled=True),
    )
    collected = (
        lax.all_gather(blocked[0], "tp", axis=0, tiled=True),
        lax.all_gather(blocked[1], "tp", axis=0, tiled=True),
        lax.all_gather(blocked[2], "tp", axis=0, tiled=True),
        lax.all_gather(blocked[3], "tp", axis=0, tiled=True),
    )
    outer_count = lax.axis_size("tp")
    inner_count = lax.axis_size("fs")
    gate_a = reorder(collected[0], outer_count, inner_count)
    up_a = reorder(collected[1], outer_count, inner_count)
    gate_b = reorder(collected[2], outer_count, inner_count)
    up_b = reorder(collected[3], outer_count, inner_count)
    down_a, down_b = (
        lax.all_gather(round_down_a, "tp", axis=1, tiled=True),
        lax.all_gather(round_down_b, "tp", axis=1, tiled=True),
    )
    tokens_in = prompts.reshape(-1, prompts.shape[-1])
    share = tokens_in.shape[0] // lax.axis_size("fs")
    act_first = activate(normalize(tokens_in), gate_a, up_a)
    selected = act_first
    summed = lax.psum_scatter(
        jnp.dot(selected, down_a, preferred_element_type=jnp.float32).astype(jnp.bfloat16),
        "fs",
        scatter_dimension=0,
        tiled=True,
    ).astype(jnp.float32)
    own_rows = lax.dynamic_slice_in_dim(tokens_in, lax.axis_index("fs") * share, share, 0)
    middle = (own_rows.astype(jnp.float32) + 0.5 * summed).astype(jnp.bfloat16)
    act_second = activate(lax.all_gather(normalize(middle), "fs", axis=0, tiled=True), gate_b, up_b)
    selected = act_second
    final_sum = lax.psum_scatter(
        jnp.dot(selected, down_b, preferred_element_type=jnp.float32).astype(jnp.bfloat16),
        "fs",
        scatter_dimension=0,
        tiled=True,
    ).astype(jnp.float32)
    finished = (middle.astype(jnp.float32) + 0.5 * final_sum).astype(jnp.bfloat16)
    return (
        gate_a,
        up_a,
        down_a,
        gate_b,
        up_b,
        down_b,
        finished.reshape(prompts.shape[0], share, prompts.shape[-1]),
    )


def solution(mesh):
    in_specs = (
        P("tp", None, None),
        P("fs"),
        P("fs", "tp"),
        P("fs", "tp"),
        P("fs", "tp"),
        P("fs"),
        P("fs", "tp"),
        P("fs", "tp"),
        P("fs", "tp"),
    )
    out_specs = (
        P(None, "fs"),
        P(None, "fs"),
        P("fs", None),
        P(None, "fs"),
        P(None, "fs"),
        P("fs", None),
        P("tp", "fs", None),
    )
    return jax.shard_map(
        per_device, mesh=mesh, in_specs=in_specs, out_specs=out_specs, check_vma=False
    )
```

profile of v0, /device:TPU:0, one launch (start us, length us, event | category | flops | bytes accessed | tf_op | source)
XLA Modules:
  0.0 561.2 jit_solution(2317630141392950479)
XLA Ops:
  7.2 0.0 all-gather.8.cloned.1.call-start
  7.2 2.1 multiply_convert_fusion.4
  9.3 15.0 %all_to_all.140 = bf16[4,64,1408]{2,1,0:T(8,128)(2,1)S(1)} all-to-all(bf16[4,64,1408]{2,1,0:T(8,128)(2,1)S(1)} %bitcast.74), channel_id=1, replica_groups=mesh['fs'=8,'tp'=4] {'tp'}, dimensions={0} | all-to-all | bytes 1441792 | tf_op jit(solution)/shard_map/all_to_all | solution.py:44
  24.3 0.6 copy.32
  24.8 0.5 all_to_all.107
  25.3 0.1 copy.33
  25.5 25.8 %all_to_all.141 = bf16[64,8,704]{2,0,1:T(8,128)(2,1)} all-to-all(bf16[64,8,704]{2,0,1:T(8,128)(2,1)S(1)} %copy.33), channel_id=1, replica_groups=mesh['fs'=8,'tp'=4] {'fs'}, dimensions={1} | all-to-all | bytes 1441792 | tf_op jit(solution)/shard_map/all_to_all | solution.py:50
  51.2 0.0 all-gather.8.cloned.1.call-update
  51.3 0.0 all-gather.10.cloned.1.call-start
  51.3 18.9 %all_to_all.142 = bf16[4,64,1408]{2,1,0:T(8,128)(2,1)S(1)} all-to-all(bf16[4,64,1408]{2,1,0:T(8,128)(2,1)S(1)} %bitcast.72), channel_id=1, replica_groups=mesh['fs'=8,'tp'=4] {'tp'}, dimensions={0} | all-to-all | bytes 1441792 | tf_op jit(solution)/shard_map/all_to_all | solution.py:45
  70.2 0.6 copy.35
  70.8 0.5 all_to_all.114
  71.2 0.1 copy.36
  71.4 23.3 %all_to_all.143 = bf16[64,8,704]{2,0,1:T(8,128)(2,1)} all-to-all(bf16[64,8,704]{2,0,1:T(8,128)(2,1)S(1)} %copy.36), channel_id=1, replica_groups=mesh['fs'=8,'tp'=4] {'fs'}, dimensions={1} | all-to-all | bytes 1441792 | tf_op jit(solution)/shard_map/all_to_all | solution.py:51
  94.7 0.0 all-gather.10.cloned.1.call-update
  94.7 0.0 all-gather.12.cloned.1.call-start
  94.8 0.9 convert_element_type.70
  95.8 0.0 reduce-scatter.3.cloned.1.call-start
  95.8 3.1 fusion
  98.9 0.0 all-gather.8.cloned.1.call-done
  98.9 2.5 copy.34
  101.4 20.1 %all-gather.10.cloned.1.call-done = bf16[2048,704]{1,0:T(8,128)(2,1)} async-done(((bf16[512,704]{1,0:T(8,128)(2,1)}), bf16[2048,704]{1,0:T(8,128)(2,1)}) %all-gather.10.cloned.1.call-update) | async-done | bytes 2883600 | tf_op jit(solution)/shard_map/all_gather | solution.py:57
  121.5 4.1 copy.37
  125.6 5.0 fusion.4
  130.6 20.1 %all-gather.12.cloned.1.call-done = bf16[704,2048]{1,0:T(8,128)(2,1)} async-done(((bf16[704,512]{1,0:T(8,128)(2,1)}), bf16[704,2048]{1,0:T(8,128)(2,1)}) %all-gather.12.cloned.1.call-update) | async-done | bytes 2883600 | tf_op jit(solution)/shard_map/all_gather | solution.py:68
  150.7 12.6 %convolution_convert_fusion.1 = bf16[1024,2048]{1,0:T(8,128)(2,1)} fusion(bf16[704,2048]{1,0:T(8,128)(2,1)} %all-gather.12.cloned.1.call-done, f32[1024,704]{0,1:T(8,128)} %fusion.4, bf16[2048,704]{1,0:T(8,128)(2,1)} %bitcast.58, bf16[1,1024,2048]{2,1,0:T(8,128)(2,1)} %param.9, f32[1024]{0:T(1024)S(1)} %add_rsqrt_fusion), kind=kOutput, calls=%fused_computation.6 | convolution fusion | flops 5918294016 | bytes 17043456 | tf_op jit(solution)/shard_map/dot_general | solution.py:76
  163.3 0.2 all-gather.14.cloned.1.call-start
  163.5 0.4 copy-done.6
  164.0 2.9 multiply_convert_fusion.2
  166.9 13.3 %all_to_all.144 = bf16[4,64,1408]{2,1,0:T(8,128)(2,1)S(1)} all-to-all(bf16[4,64,1408]{2,1,0:T(8,128)(2,1)S(1)} %bitcast.75), channel_id=1, replica_groups=mesh['fs'=8,'tp'=4] {'tp'}, dimensions={0} | all-to-all | bytes 1441792 | tf_op jit(solution)/shard_map/all_to_all | solution.py:46
  180.2 1.4 copy.38
  181.6 2.4 all_to_all.121
  184.0 1.3 copy.39
  185.3 38.9 %all_to_all.145 = bf16[64,8,704]{2,0,1:T(8,128)(2,1)} all-to-all(bf16[64,8,704]{2,0,1:T(8,128)(2,1)S(1)} %copy.39), channel_id=1, replica_groups=mesh['fs'=8,'tp'=4] {'fs'}, dimensions={1} | all-to-all | bytes 1441792 | tf_op jit(solution)/shard_map/all_to_all | solution.py:52
  224.2 0.0 all-gather.16.cloned.1.call-start
  224.3 14.4 %all_to_all.146 = bf16[4,64,1408]{2,1,0:T(8,128)(2,1)S(1)} all-to-all(bf16[4,64,1408]{2,1,0:T(8,128)(2,1)} %bitcast.73), channel_id=1, replica_groups=mesh['fs'=8,'tp'=4] {'tp'}, dimensions={0} | all-to-all | bytes 1441792 | tf_op jit(solution)/shard_map/all_to_all | solution.py:47
  238.7 1.4 copy.41
  240.1 2.4 all_to_all.128
  242.5 1.3 copy.42
  243.8 39.6 %all_to_all.147 = bf16[64,8,704]{2,0,1:T(8,128)(2,1)} all-to-all(bf16[64,8,704]{2,0,1:T(8,128)(2,1)S(1)} %copy.42), channel_id=1, replica_groups=mesh['fs'=8,'tp'=4] {'fs'}, dimensions={1} | all-to-all | bytes 1441792 | tf_op jit(solution)/shard_map/all_to_all | solution.py:53
  283.4 0.0 all-gather.20.cloned.1.call-start
  283.5 0.4 reduce-scatter.3.cloned.1.call-done
  283.9 1.5 fusion.8
  285.4 0.8 copy-done.2
  286.2 0.9 fusion.9
  287.2 0.0 all-gather.18.cloned.1.call-start
  287.2 2.3 convert_element_type.73
  289.5 0.0 reduce-scatter.5.cloned.1.call-start
  289.6 23.7 %all-gather.14.cloned.1.call-done = bf16[2048,704]{1,0:T(8,128)(2,1)} async-done(((bf16[512,704]{1,0:T(8,128)(2,1)}), bf16[2048,704]{1,0:T(8,128)(2,1)}) %all-gather.14.cloned.1.call-update) | async-done | bytes 2883600 | tf_op jit(solution)/shard_map/all_gather | solution.py:58
  313.3 3.9 copy.40
  317.2 26.1 %all-gather.16.cloned.1.call-done = bf16[2048,704]{1,0:T(8,128)(2,1)} async-done(((bf16[512,704]{1,0:T(8,128)(2,1)}), bf16[2048,704]{1,0:T(8,128)(2,1)}) %all-gather.16.cloned.1.call-update) | async-done | bytes 2883600 | tf_op jit(solution)/shard_map/all_gather | solution.py:59
  343.3 3.9 copy.43
  347.2 71.6 %all-gather.20.cloned.1.call-done = bf16[1024,2048]{1,0:T(8,128)(2,1)} async-done(((bf16[128,2048]{1,0:T(8,128)(2,1)}), bf16[1024,2048]{1,0:T(8,128)(2,1)}) %all-gather.20.cloned.1.call-update) | async-done | bytes 4194320 | tf_op jit(solution)/shard_map/all_gather | solution.py:83
  418.8 7.9 %fusion.16 = f32[1024,704]{0,1:T(8,128)} fusion(bf16[1024,2048]{1,0:T(8,128)(2,1)} %all-gather.20.cloned.1.call-done, bf16[2048,704]{1,0:T(8,128)(2,1)} %bitcast.60), kind=kOutput, calls=%fused_computation.27 | convolution fusion | flops 2952790016 | bytes 9961472 | tf_op jit(solution)/shard_map/dot_general | solution.py:14
  426.7 19.8 %all-gather.18.cloned.1.call-done = bf16[704,2048]{1,0:T(8,128)(2,1)} async-done(((bf16[704,512]{1,0:T(8,128)(2,1)}), bf16[704,2048]{1,0:T(8,128)(2,1)}) %all-gather.18.cloned.1.call-update) | async-done | bytes 2883600 | tf_op jit(solution)/shard_map/all_gather | solution.py:69
  446.5 12.2 %convolution_convert_fusion = bf16[1024,2048]{1,0:T(8,128)(2,1)} fusion(bf16[704,2048]{1,0:T(8,128)(2,1)} %all-gather.18.cloned.1.call-done, f32[1024,704]{0,1:T(8,128)} %fusion.16, bf16[1024,2048]{1,0:T(8,128)(2,1)} %all-gather.20.cloned.1.call-done, bf16[2048,704]{1,0:T(8,128)(2,1)} %bitcast.62), kind=kOutput, calls=%fused_computation.5 | convolution fusion | flops 5912002560 | bytes 17039360 | tf_op jit(solution)/shard_map/dot_general | solution.py:86
  458.7 2.7 copy.44
  461.4 4.7 copy.45
  466.2 2.7 copy.46
  468.8 4.6 copy.47
  473.5 73.7 %reduce-scatter.5.cloned.1.call-done = bf16[128,2048]{1,0:T(8,128)(2,1)} async-done(((bf16[1024,2048]{1,0:T(8,128)(2,1)}), bf16[128,2048]{1,0:T(8,128)(2,1)}) %reduce-scatter.5.cloned.1.call-update) | async-done | bytes 524304 | tf_op jit(solution)/shard_map/reduce_scatter | solution.py:85
  547.2 2.0 fusion.12
  549.2 3.9 copy.50
  553.1 1.6 copy.51
  (21 shorter events, 0.2 us)
Async XLA Ops:
  7.2 91.8 %all-gather.8.cloned.1.call-start = ((), (), s32[]{:S(2)}) async-start(), calls=%async_computation.10 | async-start | bytes 3932160 | tf_op jit(solution)/shard_map/all_gather | solution.py:56
  51.3 70.3 %all-gather.10.cloned.1.call-start = ((), (), s32[]{:S(2)}) async-start(), calls=%async_computation.11 | async-start | bytes 3932160 | tf_op jit(solution)/shard_map/all_gather | solution.py:57
  70.7 24.0 %copy-start.5 = (f32[704,512]{1,0:T(8,128)S(1)}, f32[704,512]{1,0:T(8,128)}, u32[]{:S(2)}) copy-start(f32[704,512]{1,0:T(8,128)} %param.13) | copy-start | bytes 4325380
  94.7 56.0 %all-gather.12.cloned.1.call-start = ((), (), s32[]{:S(2)}) async-start(), calls=%async_computation.12 | async-start | bytes 3604480 | tf_op jit(solution)/shard_map/all_gather | solution.py:68
  95.8 188.1 %reduce-scatter.3.cloned.1.call-start = ((), (), s32[]{:S(2)}) async-start(), calls=%async_computation.16 | async-start | bytes 4718592 | tf_op jit(solution)/shard_map/reduce_scatter | solution.py:75
  121.5 4.1 copy-start.1
  163.3 0.7 copy-start.6
  163.3 150.0 %all-gather.14.cloned.1.call-start = ((), (), s32[]{:S(2)}) async-start(), calls=%async_computation.13 | async-start | bytes 3932160 | tf_op jit(solution)/shard_map/all_gather | solution.py:58
  224.2 119.1 %all-gather.16.cloned.1.call-start = ((), (), s32[]{:S(2)}) async-start(), calls=%async_computation.14 | async-start | bytes 3932160 | tf_op jit(solution)/shard_map/all_gather | solution.py:59
  283.4 135.4 %all-gather.20.cloned.1.call-start = ((), (), s32[]{:S(2)}) async-start(), calls=%async_computation.17 | async-start | bytes 4718592 | tf_op jit(solution)/shard_map/all_gather | solution.py:83
  285.4 0.8 copy-start.2
  287.2 159.4 %all-gather.18.cloned.1.call-start = ((), (), s32[]{:S(2)}) async-start(), calls=%async_computation.15 | async-start | bytes 3604480 | tf_op jit(solution)/shard_map/all_gather | solution.py:69
  289.5 257.7 %reduce-scatter.5.cloned.1.call-start = ((), (), s32[]{:S(2)}) async-start(), calls=%async_computation.18 | async-start | bytes 4718592 | tf_op jit(solution)/shard_map/reduce_scatter | solution.py:85
  461.4 4.7 copy-start
  468.8 78.4 %copy-start.3 = (bf16[128,2048]{1,0:T(8,128)(2,1)S(1)}, bf16[128,2048]{1,0:T(8,128)(2,1)}, u32[]{:S(2)}) copy-start(bf16[128,2048]{1,0:T(8,128)(2,1)} %copy-done.2) | copy-start | bytes 1572868
  549.2 3.9 copy-start.4
Sparse Core Ops, SparseCore 0:
  51.4 31.6 all-gather.7
  94.9 26.6 all-gather.9
  123.7 27.0 all-gather.11
  163.4 120.3 reduce-scatter.2
  285.3 28.0 all-gather.13
  314.7 28.4 all-gather.15
  346.0 72.7 all-gather.19
  420.9 25.5 all-gather.17
  458.9 88.2 reduce-scatter.4
where the time goes:
time: 562 us; the launch traced here: 561 us
  waiting for transfers between devices  256 us (46%)
  blocking collectives  189 us (34%)
  local copies, waits for them, and re-layouts  48.3 us (9%)
  matrix products  37.7 us (7%)
  other arithmetic  15.8 us (3%)
  between operations  14 us (2%)
    reduce_scatter x1, waiting for transfers between devices, per_device(): lax.psum_scatter(jnp.dot(selected, down_b, preferred_element_type=jnp.flo...  73.7 us
    all_gather x1, waiting for transfers between devices, per_device(): lax.all_gather(normalize(middle), 'fs', axis=0, tiled=True)  71.6 us
    all_to_all x1, blocking collectives, per_device(): lax.all_to_all(sliced[3], 'fs', split_axis=1, concat_axis=0, tiled=True)  39.6 us
    all_to_all x1, blocking collectives, per_device(): lax.all_to_all(sliced[2], 'fs', split_axis=1, concat_axis=0, tiled=True)  38.9 us
    all_gather x1, waiting for transfers between devices, per_device(): lax.all_gather(blocked[3], 'tp', axis=0, tiled=True)  26.1 us
    all_to_all x1, blocking collectives, per_device(): lax.all_to_all(sliced[0], 'fs', split_axis=1, concat_axis=0, tiled=True)  25.8 us
    all_gather x1, waiting for transfers between devices, per_device(): lax.all_gather(blocked[2], 'tp', axis=0, tiled=True)  23.7 us
    all_to_all x1, blocking collectives, per_device(): lax.all_to_all(sliced[1], 'fs', split_axis=1, concat_axis=0, tiled=True)  23.3 us
  transfers between devices with their start and end apart: 9, of which 8 were waited for; matrix products, arithmetic and copies ran while one was open for 11% of the time, Pallas kernels for 0%

commit v1 on v0

v1 whole, which is shorter than its diff:
```python
import functools

import jax
import jax.numpy as jnp
from jax import lax
from jax.experimental import pallas as pl
from jax.experimental.pallas import tpu as pltpu
from jax.sharding import PartitionSpec as P

CORES = 2


def normalize(row_block):
    widened = row_block.astype(jnp.float32)
    scaled = widened * lax.rsqrt(jnp.mean(widened * widened, axis=-1, keepdims=True) + 1e-06)
    return scaled.astype(jnp.bfloat16)


def activate(normed, gate_cols, up_cols):
    gate_val = jnp.dot(normed, gate_cols, preferred_element_type=jnp.float32)
    up_val = jnp.dot(normed, up_cols, preferred_element_type=jnp.float32)
    return (jax.nn.silu(gate_val) * up_val).astype(jnp.bfloat16)


def partner(index, step, count):
    if count & (count - 1):
        return (index + step) % count
    result, bit = 0, 1
    while bit < count:
        result = result + ((index // bit + step // bit) % 2) * bit
        bit *= 2
    return result


def exchange_kernel(n_fs, n_tp, has_down, *refs):
    if has_down:
        (gu, dn, gu_out, dn_out, send_a, recv_a, send_y, recv_y, send_m, recv_m,
         dn_local, dn_send_y, dn_recv_y, dn_send_m, dn_recv_m) = refs
    else:
        gu, gu_out, send_a, recv_a, send_y, recv_y, send_m, recv_m = refs
    per = n_fs // n_tp
    n_y = n_tp // CORES
    rows = gu.shape[2]
    part = rows // n_tp
    me_f, me_t = lax.axis_index("fs"), lax.axis_index("tp")
    my_y, my_c = me_t // CORES, me_t % CORES
    mate = my_y * CORES + (1 - my_c)
    holder = me_f // per
    is_self = holder == me_t

    def peer_y(step):
        return (my_y + step) % n_y

    def window(f, q):
        return gu_out.at[:, pl.ds(pl.multiple_of(f * rows + q * part, part), part), :]

    def remote(src, dst, send, recv, f, t):
        return pltpu.make_async_remote_copy(
            src_ref=src, dst_ref=dst, send_sem=send, recv_sem=recv,
            device_id={"fs": f, "tp": t}, device_id_type=pl.DeviceIdType.MESH,
        )

    barrier = pltpu.get_barrier_semaphore()

    def greet(f, t):
        pl.semaphore_signal(
            barrier, inc=1, device_id={"fs": f, "tp": t}, device_id_type=pl.DeviceIdType.MESH
        )

    for step in range(n_fs):
        f = partner(me_f, step, n_fs)
        if step == 0:
            @pl.when(jnp.logical_not(is_self))
            def _():
                greet(f, holder)
        else:
            greet(f, holder)
    for step in range(1, n_y):
        greet(me_f, peer_y(step) * CORES + my_c)
    greet(me_f, mate)
    pl.semaphore_wait(barrier, per * n_tp + n_y - jnp.where(is_self, 1, 0))

    def first(i, step):
        q = (me_t + step) % n_tp
        f = me_t * per + i
        src = gu.at[:, i, pl.ds(pl.multiple_of(q * part, part), part), :]
        dst = window(me_f, q)
        copy = remote(src, dst, send_a.at[i * n_tp + step], recv_a.at[me_f], f, q)
        return copy, src, dst, f == me_f

    for step in range(n_tp - 1, -1, -1):
        for i in range(per):
            copy, src, dst, here = first(i, step)
            if step == 0:
                @pl.when(here)
                def _():
                    pltpu.make_async_copy(src, dst, recv_a.at[me_f]).start()

                @pl.when(jnp.logical_not(here))
                def _():
                    copy.start()
            else:
                copy.start()

    if has_down:
        width = dn.shape[1]

        def columns(t):
            return dn_out.at[:, pl.ds(pl.multiple_of(t * width, 128), width)]

        keep = pltpu.make_async_copy(dn, columns(me_t), dn_local)
        keep.start()
        dn_sends = []
        for step in range(1, n_y):
            dn_sends.append(remote(dn, columns(me_t), dn_send_y.at[step], dn_recv_y.at[my_y],
                                   me_f, peer_y(step) * CORES + my_c))
        dn_sends.append(remote(dn, columns(me_t), dn_send_m.at[0], dn_recv_m.at[my_y], me_f, mate))
        for copy in dn_sends:
            copy.start()

    sends = []
    for step in range(n_fs):
        f = partner(me_f, step, n_fs)
        piece = window(f, me_t)
        remote(piece, piece, send_m.at[0], recv_a.at[f], me_f, mate).wait_recv()
        for hop in range(1, n_y):
            sends.append(remote(piece, piece, send_y.at[(hop - 1) * n_fs + step],
                                recv_y.at[my_y * n_fs + f], me_f, peer_y(hop) * CORES + my_c))
            sends[-1].start()
        sends.append(remote(piece, piece, send_m.at[step], recv_m.at[my_y * n_fs + f], me_f, mate))
        sends[-1].start()

    if has_down:
        for hop in range(1, n_y):
            y = peer_y(hop)
            block = columns(y * CORES + my_c)
            copy = remote(block, block, dn_send_m.at[hop], dn_recv_m.at[y], me_f, mate)
            remote(block, block, dn_send_m.at[hop], dn_recv_y.at[y], me_f, mate).wait_recv()
            copy.start()
            dn_sends.append(copy)

    for step in range(n_fs):
        f = partner(me_f, step, n_fs)
        for hop in range(1, n_y):
            y = peer_y(hop)
            piece = window(f, y * CORES + my_c)
            send = send_m.at[hop * n_fs + step]
            remote(piece, piece, send, recv_y.at[y * n_fs + f], me_f, mate).wait_recv()
            sends.append(remote(piece, piece, send, recv_m.at[y * n_fs + f], me_f, mate))
            sends[-1].start()

    for hop in range(n_y):
        y = peer_y(hop)
        for step in range(n_fs):
            f = partner(me_f, step, n_fs)
            piece = window(f, y * CORES + (1 - my_c))
            remote(piece, piece, send_m.at[0], recv_m.at[y * n_fs + f], me_f, mate).wait_recv()
        if has_down:
            block = columns(y * CORES + (1 - my_c))
            remote(block, block, dn_send_m.at[0], dn_recv_m.at[y], me_f, mate).wait_recv()

    for copy in sends:
        copy.wait_send()
    for i in range(per):
        for step in range(n_tp):
            copy, _, _, here = first(i, step)
            if step == 0:
                @pl.when(jnp.logical_not(here))
                def _():
                    copy.wait_send()
            else:
                copy.wait_send()
    if has_down:
        keep.wait()
        for copy in dn_sends:
            copy.wait_send()


def exchange(stacked, down, collective_id):
    n_fs, n_tp = lax.axis_size("fs"), lax.axis_size("tp")
    n_y = n_tp // CORES
    kinds, per, rows, cols = stacked.shape
    has_down = down is not None
    dma = pltpu.SemaphoreType.DMA
    scratch = [dma((per * n_tp,)), dma((n_fs,)), dma((n_y * n_fs,)), dma((n_y * n_fs,)),
               dma((n_y * n_fs,)), dma((n_y * n_fs,))]
    outs = [jax.ShapeDtypeStruct((kinds, n_fs * rows, cols), stacked.dtype)]
    operands = [stacked]
    if has_down:
        scratch += [dma, dma((n_y,)), dma((n_y,)), dma((n_y,)), dma((n_y,))]
        outs.append(jax.ShapeDtypeStruct((down.shape[0], n_tp * down.shape[1]), down.dtype))
        operands.append(down)
    total = sum(out.size * 2 for out in outs)
    return pl.pallas_call(
        functools.partial(exchange_kernel, n_fs, n_tp, has_down),
        out_shape=outs,
        in_specs=[pl.BlockSpec(memory_space=pltpu.VMEM)] * len(operands),
        out_specs=[pl.BlockSpec(memory_space=pl.ANY)] * len(outs),
        scratch_shapes=scratch,
        compiler_params=pltpu.CompilerParams(
            collective_id=collective_id, has_side_effects=True, vmem_limit_bytes=16 * 2**20
        ),
        cost_estimate=pl.CostEstimate(flops=0, bytes_accessed=total * 24, transcendentals=0),
    )(*operands)


def per_device(
    prompts,
    gain_first,
    gate_first,
    up_first,
    down_first,
    gain_second,
    gate_second,
    up_second,
    down_second,
):
    per = lax.axis_size("fs") // lax.axis_size("tp")

    def fold(gain, *matrices):
        blocks = []
        for matrix in matrices:
            folded = (gain[:, None] * matrix).astype(jnp.bfloat16)
            width = folded.shape[1] // per
            blocks.append(jnp.stack([folded[:, i * width:(i + 1) * width] for i in range(per)]))
        return jnp.stack(blocks)

    served_a, down_a = exchange(
        fold(gain_first, gate_first, up_first), down_first.astype(jnp.bfloat16), 0
    )
    gate_a, up_a = served_a[0], served_a[1]

    tokens_in = prompts.reshape(-1, prompts.shape[-1])
    share = tokens_in.shape[0] // lax.axis_size("fs")
    act_first = activate(normalize(tokens_in), gate_a, up_a)
    branch = jnp.dot(act_first, down_a, preferred_element_type=jnp.float32).astype(jnp.bfloat16)

    stack_b = fold(gain_second, gate_second, up_second)
    round_b = down_second.astype(jnp.bfloat16)
    stack_b, round_b, branch = lax.optimization_barrier((stack_b, round_b, branch))
    gate_stack_b, down_b = exchange(stack_b[:1], round_b, 1)
    summed = lax.psum_scatter(branch, "fs", scatter_dimension=0, tiled=True)
    summed, gate_stack_b, down_b = lax.optimization_barrier((summed, gate_stack_b, down_b))
    summed = summed.astype(jnp.float32)
    own_rows = lax.dynamic_slice_in_dim(tokens_in, lax.axis_index("fs") * share, share, 0)
    middle = (own_rows.astype(jnp.float32) + 0.5 * summed).astype(jnp.bfloat16)
    normed = normalize(middle)
    up_in, normed = lax.optimization_barrier((stack_b[1:], normed))
    (up_stack_b,) = exchange(up_in, None, 2)
    gathered = lax.all_gather(normed, "fs", axis=0, tiled=True)
    gate_b, up_b = gate_stack_b[0], up_stack_b[0]
    act_second = activate(gathered, gate_b, up_b)
    final_sum = lax.psum_scatter(
        jnp.dot(act_second, down_b, preferred_element_type=jnp.float32).astype(jnp.bfloat16),
        "fs",
        scatter_dimension=0,
        tiled=True,
    ).astype(jnp.float32)
    finished = (middle.astype(jnp.float32) + 0.5 * final_sum).astype(jnp.bfloat16)
    return (
        gate_a,
        up_a,
        down_a,
        gate_b,
        up_b,
        down_b,
        finished.reshape(prompts.shape[0], share, prompts.shape[-1]),
    )


def solution(mesh):
    in_specs = (
        P("tp", None, None),
        P("fs"),
        P("fs", "tp"),
        P("fs", "tp"),
        P("fs", "tp"),
        P("fs"),
        P("fs", "tp"),
        P("fs", "tp"),
        P("fs", "tp"),
    )
    out_specs = (
        P(None, "fs"),
        P(None, "fs"),
        P("fs", None),
        P(None, "fs"),
        P(None, "fs"),
        P("fs", None),
        P("tp", "fs", None),
    )
    return jax.shard_map(
        per_device, mesh=mesh, in_specs=in_specs, out_specs=out_specs, check_vma=False
    )
```

time: 562 us -> 461 us (0.82)
  Pallas kernels: 0 us -> 227 us
  blocking collectives: 189 us -> 0 us
  waiting for transfers between devices: 256 us -> 136 us
  local copies, waits for them, and re-layouts: 48.3 us -> 34.1 us
    pallas_call x0 -> x3, Pallas kernels: none -> 227 us  [exchange(): pl.pallas_call(functools.partial(exchange_kernel, n_fs, n_tp, has_down),...]
    all_to_all x8 -> x0, blocking collectives: 189 us -> none  [the longest x1 39.6 us: per_device(): lax.all_to_all(sliced[3], 'fs', split_axis=1, concat_axis=0, tiled=True)]
    all_gather x7 -> x1, waiting for transfers between devices: 181 us -> 31.1 us  [per_device(): gathered = lax.all_gather(normed, 'fs', axis=0, tiled=True)]
    reduce_scatter x2, waiting for transfers between devices: 74.1 us -> 105 us  [the longest x1 65 us: per_device(): lax.psum_scatter(jnp.dot(act_second, down_b, preferred_element_type=jnp.f...]
    transpose x4 -> x0, local copies, waits for them, and re-layouts: 14.3 us -> none  [reorder(): return jnp.transpose(shaped, (1, 0, 2, 3)).reshape(total_rows, columns)]
    all_to_all x12 -> x0, local copies, waits for them, and re-layouts: 12.5 us -> none  [the longest x2 3.7 us: per_device(): lax.all_to_all(sliced[2], 'fs', split_axis=1, concat_axis=0, tiled=True)]
    squeeze x0 -> x1, local copies, waits for them, and re-layouts: none -> 5.88 us  [per_device(): gate_a, up_a = (served_a[0], served_a[1])]
    unnamed x20 -> x38, local copies, waits for them, and re-layouts: 21.4 us -> 26.3 us
  transfers between devices with their start and end apart: 9 -> 3, of which waited for: 8 -> 3; matrix products, arithmetic and copies ran while one was open for 11% -> 5% of each run, Pallas kernels for 0% -> 30%
where the time goes in v1:
time: 461 us; the launch traced here: 460 us
  Pallas kernels  227 us (49%)
  waiting for transfers between devices  136 us (30%)
  matrix products  36 us (8%)
  local copies, waits for them, and re-layouts  34.1 us (7%)
  between operations  14 us (3%)
  other arithmetic  13.1 us (3%)
    pallas_call x3, Pallas kernels, exchange(): pl.pallas_call(functools.partial(exchange_kernel, n_fs, n_tp, has_down),...  227 us
    reduce_scatter x1, waiting for transfers between devices, per_device(): lax.psum_scatter(jnp.dot(act_second, down_b, preferred_element_type=jnp.f...  65 us
    reduce_scatter x1, waiting for transfers between devices, per_device(): summed = lax.psum_scatter(branch, 'fs', scatter_dimension=0, tiled=True)  39.6 us
    all_gather x1, waiting for transfers between devices, per_device(): gathered = lax.all_gather(normed, 'fs', axis=0, tiled=True)  31.1 us
    unnamed x38, local copies, waits for them, and re-layouts  26.3 us
    dot_general x2, matrix products, activate(): gate_val = jnp.dot(normed, gate_cols, preferred_element_type=jnp.float32)  13 us
    dot_general x1, matrix products, per_device(): jnp.dot(act_first, down_a, preferred_element_type=jnp.float32)  11.8 us
    dot_general x1, matrix products, per_device(): jnp.dot(act_second, down_b, preferred_element_type=jnp.float32)  11.2 us
  transfers between devices with their start and end apart: 3, of which 3 were waited for; matrix products, arithmetic and copies ran while one was open for 5% of the time, Pallas kernels for 30%

profile of v1, /device:TPU:0, one launch (start us, length us, event | category | flops | bytes accessed | tf_op | source)
XLA Modules:
  0.0 460.0 jit_solution(10748262596800284839)
XLA Ops:
  7.2 0.0 copy-start.13
  7.2 0.0 reduce-scatter.3.cloned.1.call-start
  7.2 1.6 convert_element_type.70.refs_1_
  8.8 0.0 copy-start.11
  8.8 0.0 copy-start.12
  8.8 0.0 copy-start.14
  8.8 3.2 fusion
  12.1 0.0 copy-done.13
  12.1 0.9 convert_element_type.73.refs_1_
  13.0 0.0 copy-done.11
  13.0 0.0 copy-done.12
  13.0 0.0 copy-done.14
  13.0 0.3 multiply_convert_fusion.5
  13.3 0.5 slice_bitcast_fusion.7
  13.7 0.1 maximum_bitcast_fusion
  13.8 0.1 maximum_bitcast_fusion.1
  13.9 0.0 copy-start.8
  13.9 0.2 pad_maximum_fusion.refs_0_
  14.1 88.8 %shard_map.144 = (bf16[2,2048,704]{2,1,0:T(8,128)(2,1)S(1)}, bf16[704,2048]{1,0:T(8,128)(2,1)S(1)}) custom-call(bf16[2,2,256,704]{3,2,1,0:T(8,128)(2,1)S(1)} %pad_maximum_fusion.refs_0_, bf16[704,512]{1,0:T(8,128)(2,1)S(1)} %convert_element_type.70.refs_1_), custom_call_target="tpu_custom_call" | custom-call | bytes 207618048 | tf_op jit(solution)/shard_map/pallas_call | solution.py:194
  102.9 0.0 copy-start
  102.9 0.0 copy-start.3
  102.9 0.0 copy-done.8
  102.9 5.1 %fusion.4 = f32[1024,704]{0,1:T(8,128)} fusion(bf16[1,1024,2048]{2,1,0:T(8,128)(2,1)S(1)} %copy-done.8, f32[1024]{0:T(1024)S(1)} %add_rsqrt_fusion, bf16[2,2048,704]{2,1,0:T(8,128)(2,1)S(1)} %get-tuple-element.19), kind=kOutput, calls=%fused_computation.11 | convolution fusion | flops 2959081472 | bytes 10227712 | tf_op jit(solution)/shard_map/dot_general | solution.py:20
  108.0 0.0 copy-done
  108.0 11.8 %convolution_convert_fusion.1 = bf16[1024,2048]{1,0:T(8,128)(2,1)} fusion(bf16[704,2048]{1,0:T(8,128)(2,1)S(1)} %get-tuple-element.69, f32[1024,704]{0,1:T(8,128)} %fusion.4, bf16[1,1024,2048]{2,1,0:T(8,128)(2,1)} %param.9, f32[1024]{0:T(1024)S(1)} %add_rsqrt_fusion, bf16[2,2048,704]{2,1,0:T(8,128)(2,1)} %copy-done), kind=kOutput, calls=%fused_computation.6 | convolution fusion | flops 5918294016 | bytes 17305600 | tf_op jit(solution)/shard_map/dot_general | solution.py:236
  119.8 2.1 multiply_convert_fusion.3
  121.8 0.5 slice_bitcast_fusion.3
  122.3 0.1 maximum_bitcast_fusion.2
  122.4 0.1 maximum_bitcast_fusion.3
  122.5 0.2 pad_maximum_fusion.1
  122.6 0.0 copy-start.7
  122.6 0.0 reduce-scatter.3.cloned.1.call-update
  122.7 0.0 all-gather.2.cloned.1.call-start
  122.7 1.0 fusion.20
  123.7 0.1 copy-done.7
  123.8 77.3 %shard_map.145 = (bf16[1,2048,704]{2,1,0:T(8,128)(2,1)S(1)}, bf16[704,2048]{1,0:T(8,128)(2,1)S(1)}) custom-call(bf16[1,2,256,704]{3,2,1,0:T(8,128)(2,1)S(1)} %get-tuple-element.43.refs_0_, bf16[704,512]{1,0:T(8,128)(2,1)S(1)} %copy-done.7), custom_call_target="tpu_custom_call" | custom-call | bytes 138412032 | tf_op jit(solution)/shard_map/pallas_call | solution.py:194
  201.1 0.0 copy-start.1
  201.1 1.6 copy-done.1
  202.8 1.6 copy-done.5
  204.3 39.6 %reduce-scatter.3.cloned.1.call-done = bf16[128,2048]{1,0:T(8,128)(2,1)} async-done(((bf16[1024,2048]{1,0:T(8,128)(2,1)}), bf16[128,2048]{1,0:T(8,128)(2,1)}) %reduce-scatter.3.cloned.1.call-update) | async-done | bytes 524304 | tf_op jit(solution)/shard_map/reduce_scatter | solution.py:242
  243.9 1.5 fusion.8
  245.4 0.0 copy-start.9
  245.4 0.8 copy-done.9
  246.2 0.9 fusion.9
  247.2 0.0 all-gather.2.cloned.1.call-update
  247.2 0.0 reduce-scatter.5.cloned.1.call-start
  247.2 0.0 copy-start.2
  247.2 1.1 copy-done.2
  248.4 60.8 %shard_map.146 = bf16[1,2048,704]{2,1,0:T(8,128)(2,1)S(1)} custom-call(bf16[1,2,256,704]{3,2,1,0:T(8,128)(2,1)S(1)} %copy-done.2), custom_call_target="tpu_custom_call" | custom-call | bytes 69206016 | tf_op jit(solution)/shard_map/pallas_call | solution.py:194
  309.1 31.1 %all-gather.2.cloned.1.call-done = bf16[1024,2048]{1,0:T(8,128)(2,1)} async-done(((bf16[128,2048]{1,0:T(8,128)(2,1)}), bf16[1024,2048]{1,0:T(8,128)(2,1)}) %all-gather.2.cloned.1.call-update) | async-done | bytes 4194320 | tf_op jit(solution)/shard_map/all_gather | solution.py:250
  340.3 7.9 %fusion.15 = f32[1024,704]{0,1:T(8,128)} fusion(bf16[1024,2048]{1,0:T(8,128)(2,1)} %all-gather.2.cloned.1.call-done, bf16[1,2048,704]{2,1,0:T(8,128)(2,1)} %copy-done.1), kind=kOutput, calls=%fused_computation.42 | convolution fusion | flops 2952790016 | bytes 9961472 | tf_op jit(solution)/shard_map/dot_general | solution.py:20
  348.2 11.2 %convolution_convert_fusion = bf16[1024,2048]{1,0:T(8,128)(2,1)} fusion(bf16[704,2048]{1,0:T(8,128)(2,1)} %copy-done.5, f32[1024,704]{0,1:T(8,128)} %fusion.15, bf16[1024,2048]{1,0:T(8,128)(2,1)} %all-gather.2.cloned.1.call-done, bf16[1,2048,704]{2,1,0:T(8,128)(2,1)S(1)} %shard_map.146), kind=kOutput, calls=%fused_computation.5 | convolution fusion | flops 5912002560 | bytes 17039360 | tf_op jit(solution)/shard_map/dot_general | solution.py:254
  359.4 0.0 reduce-scatter.5.cloned.1.call-update
  359.5 5.9 %slice_bitcast_fusion = (bf16[2048,704]{1,0:T(8,128)(2,1)}, bf16[2048,704]{1,0:T(8,128)(2,1)}) fusion(bf16[2,2048,704]{2,1,0:T(8,128)(2,1)} %copy-done), kind=kLoop, calls=%fused_computation.7 | loop fusion | bytes 11534336 | tf_op jit(solution)/shard_map/squeeze | solution.py:231
  365.3 4.7 %copy.16 = bf16[2048,704]{0,1:T(8,128)(2,1)} copy(bf16[2048,704]{1,0:T(8,128)(2,1)} %get-tuple-element.41) | data formatting | bytes 5767168
  370.0 4.6 copy.17
  374.6 2.7 copy.19
  377.3 4.7 %copy.18 = bf16[2048,704]{0,1:T(8,128)(2,1)} copy(bf16[2048,704]{1,0:T(8,128)(2,1)} %bitcast.55) | data formatting | bytes 5767168
  382.0 65.0 %reduce-scatter.5.cloned.1.call-done = bf16[128,2048]{1,0:T(8,128)(2,1)} async-done(((bf16[1024,2048]{1,0:T(8,128)(2,1)}), bf16[128,2048]{1,0:T(8,128)(2,1)}) %reduce-scatter.5.cloned.1.call-update) | async-done | bytes 524304 | tf_op jit(solution)/shard_map/reduce_scatter | solution.py:253
  447.0 0.0 copy-done.10
  447.0 2.0 fusion.12
  449.0 1.6 copy.22
  450.6 1.3 copy-done.6
  451.9 1.6 copy.23
  (10 shorter events, 0.0 us)
Async XLA Ops:
  7.2 4.9 %copy-start.13 = (f32[704,512]{1,0:T(8,128)S(1)}, f32[704,512]{1,0:T(8,128)}, u32[]{:S(2)}) copy-start(f32[704,512]{1,0:T(8,128)} %param.17) | copy-start | bytes 4325380
  7.2 236.7 %reduce-scatter.3.cloned.1.call-start = ((), (), s32[]{:S(2)}) async-start(), calls=%async_computation.2 | async-start | bytes 4718592 | tf_op jit(solution)/shard_map/reduce_scatter | solution.py:242
  8.8 4.2 copy-start.11
  8.8 4.2 copy-start.12
  8.8 4.2 copy-start.14
  13.9 89.0 %copy-start.8 = (bf16[1,1024,2048]{2,1,0:T(8,128)(2,1)S(1)}, bf16[1,1024,2048]{2,1,0:T(8,128)(2,1)}, u32[]{:S(2)}) copy-start(bf16[1,1024,2048]{2,1,0:T(8,128)(2,1)} %param.9) | copy-start | bytes 12582916
  102.9 5.1 %copy-start = (bf16[2,2048,704]{2,1,0:T(8,128)(2,1)}, bf16[2,2048,704]{2,1,0:T(8,128)(2,1)S(1)}, u32[]{:S(2)}) copy-start(bf16[2,2048,704]{2,1,0:T(8,128)(2,1)S(1)} %get-tuple-element.19) | copy-start | bytes 17301508
  102.9 5.1 %copy-start.3 = (bf16[704,2048]{1,0:T(8,128)(2,1)}, bf16[704,2048]{1,0:T(8,128)(2,1)S(1)}, u32[]{:S(2)}) copy-start(bf16[704,2048]{1,0:T(8,128)(2,1)S(1)} %get-tuple-element.69) | copy-start | bytes 8650756
  108.0 11.8 %copy-start.15 = (f32[256]{0:T(256)S(1)}, f32[256]{0:T(256)}, u32[]{:S(2)}) copy-start(f32[256]{0:T(256)} %param.14) | copy-start | bytes 3076
  122.6 1.1 copy-start.7
  122.7 217.6 %all-gather.2.cloned.1.call-start = ((), (), s32[]{:S(2)}) async-start(), calls=%async_computation.3 | async-start | bytes 4718592 | tf_op jit(solution)/shard_map/all_gather | solution.py:250
  201.1 1.7 copy-start.1
  202.8 1.6 copy-start.5
  245.4 0.8 copy-start.9
  247.2 199.9 %reduce-scatter.5.cloned.1.call-start = ((), (), s32[]{:S(2)}) async-start(), calls=%async_computation.4 | async-start | bytes 4718592 | tf_op jit(solution)/shard_map/reduce_scatter | solution.py:253
  247.2 1.1 copy-start.2
  377.3 69.8 %copy-start.10 = (bf16[128,2048]{1,0:T(8,128)(2,1)S(1)}, bf16[128,2048]{1,0:T(8,128)(2,1)}, u32[]{:S(2)}) copy-start(bf16[128,2048]{1,0:T(8,128)(2,1)} %copy-done.9) | copy-start | bytes 1572868
  377.3 71.8 %copy-start.4 = (bf16[704,2048]{1,0:T(8,128)(2,1)S(1)}, bf16[704,2048]{1,0:T(8,128)(2,1)}, u32[]{:S(2)}) copy-start(bf16[704,2048]{1,0:T(8,128)(2,1)} %copy-done.3) | copy-start | bytes 8650756
  449.0 2.9 copy-start.6
Sparse Core Ops, SparseCore 0:
  122.8 121.0 reduce-scatter.2
  247.3 92.9 all-gather.1
  359.6 87.4 reduce-scatter.4

commit v2 on v1

--- a/solution.py
+++ b/solution.py
@@ -204,6 +204,133 @@
     )(*operands)
 
 
+def gather_kernel(n_z, n_x, cuts, blk, out, local, send_z, recv_z, send_x, recv_x):
+    share = blk.shape[0]
+    part = share // cuts
+    me_f, me_t = lax.axis_index("fs"), lax.axis_index("tp")
+    z, x = me_f // n_x, me_f % n_x
+
+    def window(zs, xs, s):
+        start = (zs * n_x + xs) * share + s * part
+        return out.at[pl.ds(pl.multiple_of(start, part), part), :]
+
+    def remote(src, dst, send, recv, f):
+        return pltpu.make_async_remote_copy(
+            src_ref=src, dst_ref=dst, send_sem=send, recv_sem=recv,
+            device_id={"fs": f, "tp": me_t}, device_id_type=pl.DeviceIdType.MESH,
+        )
+
+    has_next = (z < n_z - 1, z > 0)
+    toward = (1, -1)
+    barrier = pltpu.get_barrier_semaphore()
+
+    def greet(f):
+        pl.semaphore_signal(
+            barrier, inc=1, device_id={"fs": f, "tp": me_t}, device_id_type=pl.DeviceIdType.MESH
+        )
+
+    for way in range(2):
+        @pl.when(has_next[way])
+        def _():
+            greet(me_f + toward[way] * n_x)
+    for off in range(1, n_x):
+        greet(z * n_x + (x + off) % n_x)
+    pl.semaphore_wait(
+        barrier, n_x - 1 + jnp.where(has_next[0], 1, 0) + jnp.where(has_next[1], 1, 0)
+    )
+
+    def source(k, s, zs):
+        piece = window(zs, x, s)
+        return (blk.at[pl.ds(s * part, part), :] if k == 0 else piece), piece
+
+    def along_z(way, k, s, zs):
+        src, piece = source(k, s, zs)
+        return remote(src, piece, send_z.at[(way * n_z + k) * cuts + s],
+                      recv_z.at[(way * n_z + k + 1) * cuts + s], me_f + toward[way] * n_x)
+
+    def along_x(off, k, s, zs):
+        src, piece = source(k, s, zs)
+        return remote(src, piece, send_x.at[(off * n_z + zs) * cuts + s],
+                      recv_x.at[(off * n_z + zs) * cuts + s], z * n_x + (x + off) % n_x)
+
+    keep = pltpu.make_async_copy(blk, out.at[pl.ds(pl.multiple_of(me_f * share, share), share), :],
+                                 local)
+    keep.start()
+    for s in range(cuts):
+        for way in range(2):
+            @pl.when(has_next[way])
+            def _():
+                along_z(way, 0, s, z).start()
+        for off in range(1, n_x):
+            along_x(off, 0, s, z).start()
+
+    def each_arrival(body):
+        for k in range(1, n_z):
+            for s in range(cuts):
+                for way in range(2):
+                    zs = z - k * toward[way]
+                    inside = (z >= k) if way == 0 else (z + k < n_z)
+
+                    @pl.when(inside)
+                    def _():
+                        body(way, k, s, zs)
+
+    def pass_on(way, k, s, zs):
+        piece = window(zs, x, s)
+        remote(piece, piece, send_z.at[0], recv_z.at[(way * n_z + k) * cuts + s],
+               me_f - toward[way] * n_x).wait_recv()
+
+        @pl.when(has_next[way])
+        def _():
+            along_z(way, k, s, zs).start()
+        for off in range(1, n_x):
+            along_x(off, k, s, zs).start()
+
+    each_arrival(pass_on)
+    for zs in range(n_z):
+        for off in range(1, n_x):
+            for s in range(cuts):
+                piece = window(zs, (x + n_x - off) % n_x, s)
+                remote(piece, piece, send_x.at[0], recv_x.at[(off * n_z + zs) * cuts + s],
+                       z * n_x + (x + off) % n_x).wait_recv()
+
+    def sent(way, k, s, zs):
+        @pl.when(has_next[way])
+        def _():
+            along_z(way, k, s, zs).wait_send()
+        for off in range(1, n_x):
+            along_x(off, k, s, zs).wait_send()
+
+    each_arrival(sent)
+    for s in range(cuts):
+        for way in range(2):
+            @pl.when(has_next[way])
+            def _():
+                along_z(way, 0, s, z).wait_send()
+        for off in range(1, n_x):
+            along_x(off, 0, s, z).wait_send()
+    keep.wait()
+
+
+def gather_rows(block, collective_id):
+    n_fs = lax.axis_size("fs")
+    n_x = lax.axis_size("tp") // CORES
+    n_z = n_fs // n_x
+    cuts = 2
+    dma = pltpu.SemaphoreType.DMA
+    return pl.pallas_call(
+        functools.partial(gather_kernel, n_z, n_x, cuts),
+        out_shape=jax.ShapeDtypeStruct((n_fs * block.shape[0], block.shape[1]), block.dtype),
+        in_specs=[pl.BlockSpec(memory_space=pltpu.VMEM)],
+        out_specs=pl.BlockSpec(memory_space=pl.ANY),
+        scratch_shapes=[dma, dma((2 * (n_z + 1) * cuts,)), dma((2 * (n_z + 1) * cuts,)),
+                        dma((n_x * n_z * cuts,)), dma((n_x * n_z * cuts,))],
+        compiler_params=pltpu.CompilerParams(
+            collective_id=collective_id, has_side_effects=True, vmem_limit_bytes=16 * 2**20
+        ),
+    )(block)
+
+
 def per_device(
     prompts,
     gain_first,
@@ -238,17 +365,14 @@
     stack_b = fold(gain_second, gate_second, up_second)
     round_b = down_second.astype(jnp.bfloat16)
     stack_b, round_b, branch = lax.optimization_barrier((stack_b, round_b, branch))
-    gate_stack_b, down_b = exchange(stack_b[:1], round_b, 1)
+    served_b, down_b = exchange(stack_b, round_b, 1)
     summed = lax.psum_scatter(branch, "fs", scatter_dimension=0, tiled=True)
-    summed, gate_stack_b, down_b = lax.optimization_barrier((summed, gate_stack_b, down_b))
+    summed, served_b, down_b = lax.optimization_barrier((summed, served_b, down_b))
     summed = summed.astype(jnp.float32)
     own_rows = lax.dynamic_slice_in_dim(tokens_in, lax.axis_index("fs") * share, share, 0)
     middle = (own_rows.astype(jnp.float32) + 0.5 * summed).astype(jnp.bfloat16)
-    normed = normalize(middle)
-    up_in, normed = lax.optimization_barrier((stack_b[1:], normed))
-    (up_stack_b,) = exchange(up_in, None, 2)
-    gathered = lax.all_gather(normed, "fs", axis=0, tiled=True)
-    gate_b, up_b = gate_stack_b[0], up_stack_b[0]
+    gathered = gather_rows(normalize(middle), 2)
+    gate_b, up_b = served_b[0], served_b[1]
     act_second = activate(gathered, gate_b, up_b)
     final_sum = lax.psum_scatter(
         jnp.dot(act_second, down_b, preferred_element_type=jnp.float32).astype(jnp.bfloat16),

time: 461 us -> 437 us (0.948)
  waiting for transfers between devices: 136 us -> 86.5 us
  Pallas kernels: 227 us -> 252 us
    pallas_call x0 -> x1, Pallas kernels: none -> 48.9 us  [gather_rows(): pl.pallas_call(functools.partial(gather_kernel, n_z, n_x, cuts), out_shap...]
    all_gather x1 -> x0, waiting for transfers between devices: 31.1 us -> none  [per_device(): gathered = lax.all_gather(normed, 'fs', axis=0, tiled=True)]
    pallas_call x3 -> x2, Pallas kernels: 227 us -> 203 us  [exchange(): pl.pallas_call(functools.partial(exchange_kernel, n_fs, n_tp, has_down),...]
    reduce_scatter x1, waiting for transfers between devices: 39.6 us -> 23.4 us  [per_device(): summed = lax.psum_scatter(branch, 'fs', scatter_dimension=0, tiled=True)]
    squeeze x0 -> x1, local copies, waits for them, and re-layouts: none -> 4.93 us  [per_device(): gate_b, up_b = (served_b[0], served_b[1])]
    unnamed x38 -> x42, local copies, waits for them, and re-layouts: 26.3 us -> 27.1 us
  transfers between devices with their start and end apart: 3 -> 2, of which waited for: 3 -> 2; matrix products, arithmetic and copies ran while one was open for 5% -> 6% of each run, Pallas kernels for 30% -> 26%
where the time goes in v2:
time: 437 us; the launch traced here: 436 us
  Pallas kernels  252 us (58%)
  waiting for transfers between devices  86.5 us (20%)
  local copies, waits for them, and re-layouts  37.8 us (9%)
  matrix products  33.1 us (8%)
  between operations  14.3 us (3%)
  other arithmetic  12.5 us (3%)
    pallas_call x2, Pallas kernels, exchange(): pl.pallas_call(functools.partial(exchange_kernel, n_fs, n_tp, has_down),...  203 us
    reduce_scatter x1, waiting for transfers between devices, per_device(): lax.psum_scatter(jnp.dot(act_second, down_b, preferred_element_type=jnp.f...  63 us
    pallas_call x1, Pallas kernels, gather_rows(): pl.pallas_call(functools.partial(gather_kernel, n_z, n_x, cuts), out_shap...  48.9 us
    unnamed x42, local copies, waits for them, and re-layouts  27.1 us
    reduce_scatter x1, waiting for transfers between devices, per_device(): summed = lax.psum_scatter(branch, 'fs', scatter_dimension=0, tiled=True)  23.4 us
    dot_general x1, matrix products, per_device(): jnp.dot(act_first, down_a, preferred_element_type=jnp.float32)  11.8 us
    dot_general x1, matrix products, per_device(): jnp.dot(act_second, down_b, preferred_element_type=jnp.float32)  11.3 us
    dot_general x2, matrix products, activate(): gate_val = jnp.dot(normed, gate_cols, preferred_element_type=jnp.float32)  9.95 us
  transfers between devices with their start and end apart: 2, of which 2 were waited for; matrix products, arithmetic and copies ran while one was open for 6% of the time, Pallas kernels for 26%

profile of v2, /device:TPU:0, one launch (start us, length us, event | category | flops | bytes accessed | tf_op | source)
XLA Modules:
  0.0 436.2 jit_solution(7215970605300373845)
XLA Ops:
  7.2 0.0 copy-start.15
  7.2 0.0 reduce-scatter.3.cloned.1.call-start
  7.2 1.6 convert_element_type.70.refs_1_
  8.8 0.0 copy-start.13
  8.8 0.0 copy-start.14
  8.8 0.0 copy-start.16
  8.8 3.2 fusion
  12.1 0.0 copy-done.15
  12.1 0.9 convert_element_type.73.refs_1_
  13.0 0.0 copy-done.13
  13.0 0.0 copy-done.14
  13.0 0.0 copy-done.16
  13.0 0.3 multiply_convert_fusion.5
  13.3 0.5 slice_bitcast_fusion.9
  13.7 0.1 maximum_bitcast_fusion
  13.8 0.1 maximum_bitcast_fusion.1
  13.9 0.0 copy-start.10
  13.9 0.2 pad_maximum_fusion.refs_0_
  14.1 88.8 %shard_map.144 = (bf16[2,2048,704]{2,1,0:T(8,128)(2,1)S(1)}, bf16[704,2048]{1,0:T(8,128)(2,1)S(1)}) custom-call(bf16[2,2,256,704]{3,2,1,0:T(8,128)(2,1)S(1)} %pad_maximum_fusion.refs_0_, bf16[704,512]{1,0:T(8,128)(2,1)S(1)} %convert_element_type.70.refs_1_), custom_call_target="tpu_custom_call" | custom-call | bytes 207618048 | tf_op jit(solution)/shard_map/pallas_call | solution.py:194
  102.9 0.0 copy-start
  102.9 0.0 copy-start.4
  102.9 0.0 copy-done.10
  102.9 5.1 %fusion.4 = f32[1024,704]{0,1:T(8,128)} fusion(bf16[1,1024,2048]{2,1,0:T(8,128)(2,1)S(1)} %copy-done.10, f32[1024]{0:T(1024)S(1)} %add_rsqrt_fusion, bf16[2,2048,704]{2,1,0:T(8,128)(2,1)S(1)} %get-tuple-element.17), kind=kOutput, calls=%fused_computation.13 | convolution fusion | flops 2959081472 | bytes 10227712 | tf_op jit(solution)/shard_map/dot_general | solution.py:20
  108.0 0.0 copy-done
  108.0 0.0 copy-done.4
  108.0 11.8 %convolution_convert_fusion.1 = bf16[1024,2048]{1,0:T(8,128)(2,1)} fusion(bf16[704,2048]{1,0:T(8,128)(2,1)S(1)} %get-tuple-element.65, f32[1024,704]{0,1:T(8,128)} %fusion.4, bf16[1,1024,2048]{2,1,0:T(8,128)(2,1)} %param.9, f32[1024]{0:T(1024)S(1)} %add_rsqrt_fusion, bf16[2,2048,704]{2,1,0:T(8,128)(2,1)} %copy-done), kind=kOutput, calls=%fused_computation.6 | convolution fusion | flops 5918294016 | bytes 17305600 | tf_op jit(solution)/shard_map/dot_general | solution.py:363
  119.8 0.0 copy-done.17
  119.8 2.1 multiply_convert_fusion.3
  121.8 0.5 slice_bitcast_fusion.5
  122.3 0.1 maximum_bitcast_fusion.2
  122.4 0.1 maximum_bitcast_fusion.3
  122.5 0.2 pad_maximum_fusion.1.refs_0_
  122.6 0.0 copy-start.9
  122.6 0.0 reduce-scatter.3.cloned.1.call-update
  122.7 0.0 reduce-scatter.5.cloned.1.call-start
  122.7 1.0 copy-done.9
  123.7 114.4 %shard_map.145 = (bf16[2,2048,704]{2,1,0:T(8,128)(2,1)S(1)}, bf16[704,2048]{1,0:T(8,128)(2,1)S(1)}) custom-call(bf16[2,2,256,704]{3,2,1,0:T(8,128)(2,1)S(1)} %pad_maximum_fusion.1.refs_0_, bf16[704,512]{1,0:T(8,128)(2,1)S(1)} %copy-done.9), custom_call_target="tpu_custom_call" | custom-call | bytes 207618048 | tf_op jit(solution)/shard_map/pallas_call | solution.py:194
  238.1 0.0 copy-start.1
  238.1 2.6 copy-done.1
  240.7 1.6 copy-done.6
  242.3 23.4 %reduce-scatter.3.cloned.1.call-done = bf16[128,2048]{1,0:T(8,128)(2,1)} async-done(((bf16[1024,2048]{1,0:T(8,128)(2,1)}), bf16[128,2048]{1,0:T(8,128)(2,1)}) %reduce-scatter.3.cloned.1.call-update) | async-done | bytes 524304 | tf_op jit(solution)/shard_map/reduce_scatter | solution.py:369
  265.7 1.7 fusion.8
  267.4 0.0 copy-start.11
  267.4 0.8 copy-done.11
  268.2 0.2 fusion.9.blk
  268.3 48.9 %shard_map.146 = bf16[1024,2048]{1,0:T(8,128)(2,1)S(1)} custom-call(bf16[128,2048]{1,0:T(8,128)(2,1)S(1)} %fusion.9.blk), custom_call_target="tpu_custom_call" | custom-call | tf_op jit(solution)/shard_map/pallas_call | solution.py:321
  317.2 0.0 copy-start.3
  317.3 1.9 copy-done.3
  319.2 0.0 copy-done.2
  319.2 4.9 %fusion.15 = f32[1024,704]{0,1:T(8,128)} fusion(bf16[1024,2048]{1,0:T(8,128)(2,1)S(1)} %shard_map.146, bf16[2,2048,704]{2,1,0:T(8,128)(2,1)S(1)} %copy-done.2), kind=kOutput, calls=%fused_computation.45 | convolution fusion | flops 2952790016 | bytes 10223616 | tf_op jit(solution)/shard_map/dot_general | solution.py:20
  324.1 11.3 %convolution_convert_fusion = bf16[1024,2048]{1,0:T(8,128)(2,1)} fusion(bf16[704,2048]{1,0:T(8,128)(2,1)S(1)} %copy-done.7, f32[1024,704]{0,1:T(8,128)} %fusion.15, bf16[1024,2048]{1,0:T(8,128)(2,1)} %copy-done.3, bf16[2,2048,704]{2,1,0:T(8,128)(2,1)} %copy-done.1), kind=kOutput, calls=%fused_computation.5 | convolution fusion | flops 5912002560 | bytes 17301504 | tf_op jit(solution)/shard_map/dot_general | solution.py:378
  335.4 0.0 reduce-scatter.5.cloned.1.call-update
  335.4 4.9 %slice_bitcast_fusion.2 = (bf16[2048,704]{1,0:T(8,128)(2,1)S(1)}, bf16[2048,704]{1,0:T(8,128)(2,1)}) fusion(bf16[2,2048,704]{2,1,0:T(8,128)(2,1)} %copy-done), kind=kLoop, calls=%fused_computation.9 | loop fusion | bytes 11534336 | tf_op jit(solution)/shard_map/squeeze | solution.py:358
  340.3 4.6 %copy.16 = bf16[2048,704]{0,1:T(8,128)(2,1)} copy(bf16[2048,704]{1,0:T(8,128)(2,1)} %get-tuple-element.39) | data formatting | bytes 5767168
  344.9 2.7 copy.17
  347.6 4.9 %slice_bitcast_fusion = (bf16[2048,704]{1,0:T(8,128)(2,1)}, bf16[2048,704]{1,0:T(8,128)(2,1)S(1)}) fusion(bf16[2,2048,704]{2,1,0:T(8,128)(2,1)} %copy-done.1), kind=kLoop, calls=%fused_computation.7 | loop fusion | bytes 11534336 | tf_op jit(solution)/shard_map/squeeze | solution.py:375
  352.5 2.7 copy.18
  355.2 4.7 %copy.19 = bf16[2048,704]{0,1:T(8,128)(2,1)} copy(bf16[2048,704]{1,0:T(8,128)(2,1)} %get-tuple-element.36) | data formatting | bytes 5767168
  359.9 63.0 %reduce-scatter.5.cloned.1.call-done = bf16[128,2048]{1,0:T(8,128)(2,1)} async-done(((bf16[1024,2048]{1,0:T(8,128)(2,1)}), bf16[128,2048]{1,0:T(8,128)(2,1)}) %reduce-scatter.5.cloned.1.call-update) | async-done | bytes 524304 | tf_op jit(solution)/shard_map/reduce_scatter | solution.py:377
  423.0 2.0 fusion.12
  425.0 0.0 copy-done.5
  425.0 1.6 copy.22
  426.5 1.3 copy-done.8
  427.8 1.6 copy.23
  (11 shorter events, 0.0 us)
Async XLA Ops:
  7.2 4.9 %copy-start.15 = (f32[704,512]{1,0:T(8,128)S(1)}, f32[704,512]{1,0:T(8,128)}, u32[]{:S(2)}) copy-start(f32[704,512]{1,0:T(8,128)} %param.17) | copy-start | bytes 4325380
  7.2 258.5 %reduce-scatter.3.cloned.1.call-start = ((), (), s32[]{:S(2)}) async-start(), calls=%async_computation.2 | async-start | bytes 4718592 | tf_op jit(solution)/shard_map/reduce_scatter | solution.py:369
  8.8 4.2 copy-start.13
  8.8 4.2 copy-start.14
  8.8 4.2 copy-start.16
  13.9 89.0 %copy-start.10 = (bf16[1,1024,2048]{2,1,0:T(8,128)(2,1)S(1)}, bf16[1,1024,2048]{2,1,0:T(8,128)(2,1)}, u32[]{:S(2)}) copy-start(bf16[1,1024,2048]{2,1,0:T(8,128)(2,1)} %param.9) | copy-start | bytes 12582916
  102.9 5.1 %copy-start = (bf16[2,2048,704]{2,1,0:T(8,128)(2,1)}, bf16[2,2048,704]{2,1,0:T(8,128)(2,1)S(1)}, u32[]{:S(2)}) copy-start(bf16[2,2048,704]{2,1,0:T(8,128)(2,1)S(1)} %get-tuple-element.17) | copy-start | bytes 17301508
  102.9 5.1 %copy-start.4 = (bf16[704,2048]{1,0:T(8,128)(2,1)}, bf16[704,2048]{1,0:T(8,128)(2,1)S(1)}, u32[]{:S(2)}) copy-start(bf16[704,2048]{1,0:T(8,128)(2,1)S(1)} %get-tuple-element.65) | copy-start | bytes 8650756
  108.0 11.8 %copy-start.17 = (f32[256]{0:T(256)S(1)}, f32[256]{0:T(256)}, u32[]{:S(2)}) copy-start(f32[256]{0:T(256)} %param.14) | copy-start | bytes 3076
  122.6 1.1 copy-start.9
  122.7 300.3 %reduce-scatter.5.cloned.1.call-start = ((), (), s32[]{:S(2)}) async-start(), calls=%async_computation.3 | async-start | bytes 4718592 | tf_op jit(solution)/shard_map/reduce_scatter | solution.py:377
  238.1 2.6 copy-start.1
  240.7 1.6 copy-start.6
  265.7 53.5 %copy-start.2 = (bf16[2,2048,704]{2,1,0:T(8,128)(2,1)S(1)}, bf16[2,2048,704]{2,1,0:T(8,128)(2,1)}, u32[]{:S(2)}) copy-start(bf16[2,2048,704]{2,1,0:T(8,128)(2,1)} %copy-done.1) | copy-start | bytes 17301508
  267.4 0.8 copy-start.11
  317.2 1.9 copy-start.3
  319.2 4.9 %copy-start.7 = (bf16[704,2048]{1,0:T(8,128)(2,1)S(1)}, bf16[704,2048]{1,0:T(8,128)(2,1)}, u32[]{:S(2)}) copy-start(bf16[704,2048]{1,0:T(8,128)(2,1)} %copy-done.6) | copy-start | bytes 8650756
  355.2 67.8 %copy-start.12 = (bf16[128,2048]{1,0:T(8,128)(2,1)S(1)}, bf16[128,2048]{1,0:T(8,128)(2,1)}, u32[]{:S(2)}) copy-start(bf16[128,2048]{1,0:T(8,128)(2,1)} %copy-done.11) | copy-start | bytes 1572868
  355.2 69.8 %copy-start.5 = (bf16[704,2048]{1,0:T(8,128)(2,1)S(1)}, bf16[704,2048]{1,0:T(8,128)(2,1)}, u32[]{:S(2)}) copy-start(bf16[704,2048]{1,0:T(8,128)(2,1)} %copy-done.4) | copy-start | bytes 8650756
  425.0 2.9 copy-start.8
Sparse Core Ops, SparseCore 0:
  122.8 142.8 reduce-scatter.2
  335.5 87.3 reduce-scatter.4
